TPU v7x, 32 devices: a whole 2x2x4 slice. The times are simulated.
32 devices in a mesh: grp: 2 (over x), kv: 4 (over z), tp: 4 (over y, core).
Axes of the slice: x: 2, y: 2, z: 4, core: 2. Of those that a mesh axis runs over, the one named last changes fastest.
Arguments:
- stream: bfloat16 [32, 4096], P('grp', ('kv', 'tp')), parts along dimension 0, may hold values from -6 to 6
- attn_gain: bfloat16 [4096], P('kv'), may hold values from 0.099609375 to 1.8984375
- mlp_gain: bfloat16 [4096], P('kv'), may hold values from 0.099609375 to 1.8984375
- w_query: bfloat16 [4096, 4096], P('kv', 'tp'), may hold values from -0.09375 to 0.09375
- w_key: bfloat16 [4096, 4096], P('kv', 'tp'), may hold values from -0.09375 to 0.09375
- w_value: bfloat16 [4096, 4096], P('kv', 'tp'), may hold values from -0.09375 to 0.09375
- w_zgate: bfloat16 [4096, 4096], P('kv', 'tp'), may hold values from -0.09375 to 0.09375
- w_decay: bfloat16 [4096, 32], P('kv'), may hold values from -0.09375 to 0.09375
- w_beta: bfloat16 [4096, 32], P('kv'), may hold values from -0.09375 to 0.09375
- decay_rate: float32 [32], P('tp'), may hold values from 0.03 to 3
- head_gain: float32 [128], replicated, may hold values from 0.1 to 1.9
- w_attn_out: bfloat16 [4096, 4096], P('tp', 'kv'), may hold values from -0.09375 to 0.09375
- w_gate: bfloat16 [4096, 11264], P('kv', 'tp'), may hold values from -0.09375 to 0.09375
- w_up: bfloat16 [4096, 11264], P('kv', 'tp'), may hold values from -0.09375 to 0.09375
- w_down: bfloat16 [11264, 4096], P('tp', 'kv'), may hold values from -0.0546875 to 0.0546875
- state: float32 [32, 32, 128, 128], P(('grp', 'kv'), 'tp'), parts along dimension 0, may hold values from -4 to 4
Outputs:
- next_stream: bfloat16 [32, 4096], P('grp', ('kv', 'tp')), parts along dimension 0
- new_state: float32 [32, 32, 128, 128], P(('grp', 'kv'), 'tp'), parts along dimension 0
There are 2 independent parts, one for each index of `grp`. A program takes and returns all parts, laid end to end along the dimension named above; an argument that names none is the same for every part. Nothing has to cross between parts.
All inputs are finite; a program needn't handle non-finite values.
Results may differ from a plain program's by a relative error of at most 0.025.
Values may be sent and summed in bfloat16 or wider, within the bound.
A program may use at most 64 MiB of HBM per device.

v0:
```python
import jax
import jax.numpy as jnp
from jax import lax
from jax.sharding import PartitionSpec as P

D = 4096
HEAD_DIM = 128


EPSILON = 1e-06


def l2_unit(values):
    return values * lax.rsqrt(jnp.sum(values * values, axis=-1, keepdims=True) + EPSILON)


def delta_update(query, key_vec, value_vec, log_decay, beta_gate, state):
    decayed = jnp.exp(log_decay)[..., None, None] * state
    recalled = jnp.einsum("shkv,shk->shv", decayed, key_vec, precision=lax.Precision.HIGHEST)
    update = beta_gate[..., None] * (value_vec - recalled)
    new_state = decayed + key_vec[..., :, None] * update[..., None, :]
    head_out = jnp.einsum("shkv,shk->shv", new_state, query, precision=lax.Precision.HIGHEST)
    return (new_state, head_out)


def head_mix(head_out, head_gain, z_gate):
    scaled = head_out * lax.rsqrt(jnp.mean(head_out * head_out, axis=-1, keepdims=True) + EPSILON)
    return (scaled * head_gain * jax.nn.silu(z_gate)).astype(jnp.bfloat16)


def local(
    stream,
    attn_gain,
    mlp_gain,
    w_query,
    w_key,
    w_value,
    w_zgate,
    w_decay,
    w_beta,
    decay_rate,
    head_gain,
    w_attn_out,
    w_gate,
    w_up,
    w_down,
    state,
):
    seq_count = state.shape[0]
    local_heads = state.shape[1]
    width = w_query.shape[1]
    heads_total = w_decay.shape[1]
    kv_offset = lax.axis_index("kv") * seq_count
    head_offset = lax.axis_index("tp") * local_heads
    block_rows = lax.all_gather(stream, "tp", axis=1, tiled=True).astype(jnp.float32)
    local_squares = jnp.sum(block_rows * block_rows, axis=1)
    normed = (block_rows * attn_gain.astype(jnp.float32)[None, :]).astype(jnp.bfloat16)
    small_weights = jnp.concatenate([w_decay, w_beta], axis=1)
    pieces = [
        jnp.dot(normed, weight, preferred_element_type=jnp.float32)
        for weight in (w_query, w_key, w_value, w_zgate)
    ]
    small = jnp.dot(normed, small_weights, preferred_element_type=jnp.float32)
    own_decay = lax.dynamic_slice_in_dim(small, head_offset, local_heads, 1)
    own_beta = lax.dynamic_slice_in_dim(small, heads_total + head_offset, local_heads, 1)
    summed = lax.psum_scatter(
        jnp.concatenate(pieces + [own_decay, own_beta], axis=1).astype(jnp.bfloat16),
        "kv",
        scatter_dimension=0,
        tiled=True,
    ).astype(jnp.float32)
    total_squares = lax.psum(local_squares, "kv")
    row_scale = lax.rsqrt(total_squares / D + EPSILON)
    own_scale = lax.dynamic_slice_in_dim(row_scale, kv_offset, seq_count, 0)
    summed = summed * own_scale[:, None]

    def head_block(index):
        return summed[:, index * width : (index + 1) * width].reshape(
            seq_count, local_heads, HEAD_DIM
        )

    query = l2_unit(head_block(0)) * HEAD_DIM ** (-0.5)
    key_vec = l2_unit(head_block(1))
    value_vec = head_block(2)
    z_gate = head_block(3)
    log_decay = -decay_rate[None, :] * jax.nn.softplus(
        summed[:, 4 * width : 4 * width + local_heads]
    )
    beta_gate = jax.nn.sigmoid(summed[:, 4 * width + local_heads :])
    new_state, head_out = delta_update(query, key_vec, value_vec, log_decay, beta_gate, state)
    mixed = head_mix(head_out, head_gain, z_gate).reshape(seq_count, width)
    attn_part = jnp.dot(
        lax.all_gather(mixed, "kv", axis=0, tiled=True),
        w_attn_out,
        preferred_element_type=jnp.float32,
    )
    attn_sum = lax.psum_scatter(
        attn_part.astype(jnp.bfloat16), "tp", scatter_dimension=1, tiled=True
    ).astype(jnp.float32)
    residual_stream = (stream.astype(jnp.float32) + attn_sum).astype(jnp.bfloat16)
    mlp_block = lax.all_gather(residual_stream, "tp", axis=1, tiled=True).astype(jnp.float32)
    mlp_local_squares = jnp.sum(mlp_block * mlp_block, axis=1)
    mlp_total_squares = lax.psum(mlp_local_squares, "kv")
    normed_mlp = (mlp_block * mlp_gain.astype(jnp.float32)[None, :]).astype(jnp.bfloat16)
    gate_part = jnp.dot(normed_mlp, w_gate, preferred_element_type=jnp.float32)
    up_part = jnp.dot(normed_mlp, w_up, preferred_element_type=jnp.float32)
    operands = (gate_part, up_part)
    totals = (
        lax.psum(operands[0].astype(jnp.bfloat16), "kv").astype(jnp.float32),
        lax.psum(operands[1].astype(jnp.bfloat16), "kv").astype(jnp.float32),
    )
    gate_sum, up_sum = (totals[0], totals[1])
    mlp_scale = lax.rsqrt(mlp_total_squares / D + EPSILON)
    hidden = (jax.nn.silu(gate_sum * mlp_scale[:, None]) * (up_sum * mlp_scale[:, None])).astype(
        jnp.bfloat16
    )
    down_part = jnp.dot(hidden, w_down, preferred_element_type=jnp.float32)
    mlp_sum = lax.psum_scatter(
        down_part.astype(jnp.bfloat16), "tp", scatter_dimension=1, tiled=True
    ).astype(jnp.float32)
    next_stream = (residual_stream.astype(jnp.float32) + mlp_sum).astype(jnp.bfloat16)
    return (next_stream, new_state)


def solution(mesh):
    return jax.shard_map(
        local,
        mesh=mesh,
        in_specs=(
            P("grp", ("kv", "tp")),
            P("kv"),
            P("kv"),
            P("kv", "tp"),
            P("kv", "tp"),
            P("kv", "tp"),
            P("kv", "tp"),
            P("kv", None),
            P("kv", None),
            P("tp"),
            P(),
            P("tp", "kv"),
            P("kv", "tp"),
            P("kv", "tp"),
            P("tp", "kv"),
            P(("grp", "kv"), "tp", None, None),
        ),
        out_specs=(P("grp", ("kv", "tp")), P(("grp", "kv"), "tp", None, None)),
        check_vma=False,
    )
```

profile of v0, /device:TPU:0, one launch (start us, length us, event | category | flops | bytes accessed | tf_op | source)
XLA Modules:
  0.0 189.6 jit_solution(2436157586402226002)
XLA Ops:
  7.2 0.0 all-reduce.5.cloned.1.call-start
  7.2 0.8 convert_element_type.66
  8.1 6.6 %all_gather.9 = bf16[16,1024]{1,0:T(8,128)(2,1)S(1)} all-gather(bf16[16,256]{1,0:T(8,128)(2,1)} %param.16), channel_id=1, replica_groups=mesh['grp'=2,'kv'=4,'tp'=4] {'tp'}, dimensions={1}, use_global_device_ids=true | all-gather | bytes 40960 | tf_op jit(solution)/shard_map/all_gather | solution.py:55
  14.7 0.4 convolution_convert_fusion.6
  15.1 0.4 convolution_convert_fusion.5
  15.5 0.8 copy-done.4
  16.3 0.4 convolution_convert_fusion.4
  16.7 0.3 copy-done.5
  17.0 0.4 convolution_convert_fusion.7
  17.4 0.1 fusion.3
  17.5 0.1 dynamic-slice_convert_fusion
  17.6 0.8 concatenate.8
  18.4 0.0 all-reduce.5.cloned.1.call-update
  18.4 0.0 reduce-scatter.3.cloned.1.call-start
  18.5 0.1 fusion.10
  18.6 12.4 %psum.28 = f32[16]{0:T(128)S(1)} all-reduce(f32[16]{0:T(128)S(1)} %fusion.10), channel_id=1, replica_groups=mesh['grp'=2,'kv'=4,'tp'=4] {'kv'}, use_global_device_ids=true, to_apply=%region_2.0 | all-reduce | flops 16 | bytes 128 | tf_op jit(solution)/shard_map/psum | solution.py:72
  31.0 0.6 dynamic-slice
  32.3 0.1 dynamic_slice.11
  32.3 22.4 %all-reduce.5.cloned.1.call-done = bf16[16,4112]{1,0:T(8,128)(2,1)} async-done(((bf16[16,4112]{1,0:T(8,128)(2,1)}), bf16[16,4112]{1,0:T(8,128)(2,1)}) %all-reduce.5.cloned.1.call-update) | async-done | bytes 131600
  54.8 1.1 convert_multiply_fusion.4
  55.9 0.1 fusion.33
  56.0 0.1 fusion.22
  56.1 0.1 bitcast_multiply_fusion.3
  56.2 3.6 %fusion = f32[4,8,1,128]{3,2,1,0:T(1,128)S(1)} fusion(f32[4,8,128,1]{2,3,1,0:T(1,128)S(1)} %bitcast.62, f32[4,8,128,128]{3,2,1,0:T(8,128)} %param.31, f32[4,8]{1,0:T(4,128)S(1)} %get-tuple-element.9), kind=kOutput, calls=%fused_computation.3 | convolution fusion | flops 6815744 | bytes 2130048 | tf_op jit(solution)/shard_map/shkv,shk->shv/dot_general | solution.py:19
  59.8 0.1 fusion.19
  59.9 0.1 fusion.20
  59.9 0.7 multiply_add_fusion
  60.7 1.3 copy-done.2
  62.0 1.9 fusion.36
  63.9 0.1 multiply_reduce_fusion
  64.0 0.1 fusion.23
  64.1 13.1 %all-gather = bf16[4,4,1024]{2,1,0:T(4,128)(2,1)S(1)} all-gather(bf16[1,4,1024]{2,1,0:T(4,128)(2,1)S(1)} %reshape.59), channel_id=1, replica_groups=mesh['grp'=2,'kv'=4,'tp'=4] {'kv'}, dimensions={0}, use_global_device_ids=true | all-gather | bytes 40960 | tf_op jit(solution)/shard_map/all_gather | solution.py:93
  77.3 2.6 %convolution_convert_fusion.3 = bf16[16,1024]{1,0:T(8,128)(2,1)} fusion(bf16[16,1024]{1,0:T(8,128)(2,1)S(1)} %reshape.60, bf16[1024,1024]{1,0:T(8,128)(2,1)} %param.27), kind=kOutput, calls=%fused_computation.6 | convolution fusion | flops 33570816 | bytes 2162688 | tf_op jit(solution)/shard_map/dot_general | solution.py:92
  79.8 0.0 reduce-scatter.3.cloned.1.call-update
  79.9 0.0 all-reduce.7.cloned.1.call-start
  79.9 19.6 %reduce-scatter.3.cloned.1.call-done = bf16[16,256]{1,0:T(8,128)(2,1)} async-done(((bf16[16,1024]{1,0:T(8,128)(2,1)}), bf16[16,256]{1,0:T(8,128)(2,1)}) %reduce-scatter.3.cloned.1.call-update) | async-done | bytes 8208 | tf_op jit(solution)/shard_map/reduce_scatter | solution.py:97
  99.6 0.7 add_convert_fusion.1
  100.3 5.2 %all_gather.11 = bf16[16,1024]{1,0:T(8,128)(2,1)S(1)} all-gather(bf16[16,256]{1,0:T(8,128)(2,1)S(1)} %add_convert_fusion.1), channel_id=1, replica_groups=mesh['grp'=2,'kv'=4,'tp'=4] {'tp'}, dimensions={1}, use_global_device_ids=true | all-gather | bytes 40960 | tf_op jit(solution)/shard_map/all_gather | solution.py:101
  105.5 0.1 fusion.12
  105.6 11.7 %psum.30 = f32[16]{0:T(128)S(1)} all-reduce(f32[16]{0:T(128)S(1)} %fusion.12), channel_id=1, replica_groups=mesh['grp'=2,'kv'=4,'tp'=4] {'kv'}, use_global_device_ids=true, to_apply=%region_9.10 | all-reduce | flops 16 | bytes 128 | tf_op jit(solution)/shard_map/psum | solution.py:103
  117.3 4.1 %convolution_convert_fusion = bf16[16,2816]{1,0:T(8,128)(2,1)} fusion(bf16[1024,2816]{1,0:T(8,128)(2,1)} %param.29, bf16[16,1024]{1,0:T(8,128)(2,1)S(1)} %all_gather.11, f32[1024]{0:T(1024)S(1)} %convert_element_type.75), kind=kOutput, calls=%fused_computation | convolution fusion | flops 92368896 | bytes 5894144 | tf_op jit(solution)/shard_map/dot_general | solution.py:106
  121.4 4.1 %convolution_convert_fusion.1 = bf16[16,2816]{1,0:T(8,128)(2,1)} fusion(bf16[1024,2816]{1,0:T(8,128)(2,1)} %param.28, bf16[16,1024]{1,0:T(8,128)(2,1)S(1)} %all_gather.11, f32[1024]{0:T(1024)S(1)} %convert_element_type.75), kind=kOutput, calls=%fused_computation.1 | convolution fusion | flops 92368896 | bytes 5894144 | tf_op jit(solution)/shard_map/dot_general | solution.py:105
  125.6 0.0 all-reduce.7.cloned.1.call-update
  125.6 0.0 reduce-scatter.5.cloned.1.call-start
  125.7 32.1 %all-reduce.7.cloned.1.call-done = (bf16[16,2816]{1,0:T(8,128)(2,1)}, bf16[16,2816]{1,0:T(8,128)(2,1)}) async-done(((bf16[16,2816]{1,0:T(8,128)(2,1)}, bf16[16,2816]{1,0:T(8,128)(2,1)}), (bf16[16,2816]{1,0:T(8,128)(2,1)}, bf16[16,2816]{1,0:T(8,128)(2,1)})) %all-reduce.7.cloned.1.call-update) | async-done | bytes 180240 | tf_op jit(solution)/shard_map/psum | solution.py:110
  157.7 4.3 %convolution_convert_fusion.2 = bf16[16,1024]{1,0:T(8,128)(2,1)} fusion(bf16[2816,1024]{1,0:T(8,128)(2,1)} %param.30, bf16[16,2816]{1,0:T(8,128)(2,1)} %get-tuple-element.2, bf16[16,2816]{1,0:T(8,128)(2,1)} %get-tuple-element.3, f32[16]{0:T(128)S(1)} %add_rsqrt_fusion.3), kind=kOutput, calls=%fused_computation.5 | convolution fusion | flops 92741632 | bytes 5980224 | tf_op jit(solution)/shard_map/dot_general | solution.py:117
  162.0 19.8 %reduce-scatter.5.cloned.1.call-done = bf16[16,256]{1,0:T(8,128)(2,1)} async-done(((bf16[16,1024]{1,0:T(8,128)(2,1)}), bf16[16,256]{1,0:T(8,128)(2,1)}) %reduce-scatter.5.cloned.1.call-update) | async-done | bytes 8208 | tf_op jit(solution)/shard_map/reduce_scatter | solution.py:118
  181.8 1.3 add_convert_fusion
  (34 shorter events, 0.2 us)
Async XLA Ops:
  7.2 7.5 %copy-start = (bf16[1024,1024]{1,0:T(8,128)(2,1)S(1)}, bf16[1024,1024]{1,0:T(8,128)(2,1)}, u32[]{:S(2)}) copy-start(bf16[1024,1024]{1,0:T(8,128)(2,1)} %param.20) | copy-start | bytes 6291460
  7.2 47.6 %all-reduce.5.cloned.1.call-start = ((), (), s32[]{:S(2)}) async-start(), calls=%async_computation.4 | async-start | bytes 270336
  7.2 7.8 %copy-start.3 = (bf16[1024,1024]{1,0:T(8,128)(2,1)S(1)}, bf16[1024,1024]{1,0:T(8,128)(2,1)}, u32[]{:S(2)}) copy-start(bf16[1024,1024]{1,0:T(8,128)(2,1)} %param.21) | copy-start | bytes 6291460
  14.7 1.6 copy-start.4
  15.1 1.9 %copy-start.5 = (bf16[1024,1024]{1,0:T(8,128)(2,1)S(1)}, bf16[1024,1024]{1,0:T(8,128)(2,1)}, u32[]{:S(2)}) copy-start(bf16[1024,1024]{1,0:T(8,128)(2,1)} %param.19) | copy-start | bytes 6291460
  16.3 1.1 copy-start.9
  16.3 1.1 copy-start.10
  16.3 2.3 %copy-start.11 = (f32[8]{0:T(128)S(1)}, f32[8]{0:T(128)}, u32[]{:S(2)}) copy-start(f32[8]{0:T(128)} %param.25) | copy-start | bytes 100
  16.3 14.7 %copy-start.12 = (u32[32]{0:T(128)S(1)}, u32[32]{0:T(128)}, u32[]{:S(2)}) copy-start(u32[32]{0:T(128)} %constant.46) | copy-start | bytes 388
  18.4 81.2 %reduce-scatter.3.cloned.1.call-start = ((), (), s32[]{:S(2)}) async-start(), calls=%async_computation.2 | async-start | bytes 40960 | tf_op jit(solution)/shard_map/reduce_scatter | solution.py:97
  54.8 5.2 %copy-start.1 = (f32[4,8,128,128]{3,2,1,0:T(8,128)S(1)}, f32[4,8,128,128]{3,2,1,0:T(8,128)}, u32[]{:S(2)}) copy-start(f32[4,8,128,128]{3,2,1,0:T(8,128)} %param.31) | copy-start | bytes 6291460
  60.7 1.3 copy-start.2
  60.7 3.3 %copy-start.8 = (f32[128]{0:T(128)S(1)}, f32[128]{0:T(128)}, u32[]{:S(2)}) copy-start(f32[128]{0:T(128)} %param.26) | copy-start | bytes 1540
  62.0 17.9 %copy-start.7 = (bf16[1024]{0:T(1024)(128)(2,1)S(1)}, bf16[1024]{0:T(1024)(128)(2,1)}, u32[]{:S(2)}) copy-start(bf16[1024]{0:T(1024)(128)(2,1)} %param.18) | copy-start | bytes 6148
  62.0 37.6 %copy-start.6 = (bf16[16,256]{1,0:T(8,128)(2,1)S(1)}, bf16[16,256]{1,0:T(8,128)(2,1)}, u32[]{:S(2)}) copy-start(bf16[16,256]{1,0:T(8,128)(2,1)} %param.16) | copy-start | bytes 24580
  79.9 77.9 %all-reduce.7.cloned.1.call-start = ((), (), s32[]{:S(2)}) async-start(), calls=%async_computation.5 | async-start | bytes 360448 | tf_op jit(solution)/shard_map/psum | solution.py:110
  125.6 56.2 %reduce-scatter.5.cloned.1.call-start = ((), (), s32[]{:S(2)}) async-start(), calls=%async_computation.3 | async-start | bytes 40960 | tf_op jit(solution)/shard_map/reduce_scatter | solution.py:118
Sparse Core Ops, SparseCore 0:
  18.5 36.2 all-reduce.4
  80.0 19.5 reduce-scatter.2
  125.7 31.9 all-reduce.6
  162.1 19.5 reduce-scatter.4
where the time goes:
time: 190 us
  waiting for transfers between devices  94 us (49%)
  blocking collectives  49 us (26%)
  matrix products  22.3 us (12%)
  between operations  14.6 us (8%)
  other arithmetic  5.53 us (3%)
  local copies, waits for them, and re-layouts  4.03 us (2%)
    psum x1, waiting for transfers between devices, local(): lax.psum(operands[1].astype(jnp.bfloat16), 'kv').astype(jnp.float32)  32.1 us
    unnamed x5, waiting for transfers between devices  22.5 us
    reduce_scatter x1, waiting for transfers between devices, local(): lax.psum_scatter(down_part.astype(jnp.bfloat16), 'tp', scatter_dimension=...  19.8 us
    reduce_scatter x1, waiting for transfers between devices, local(): lax.psum_scatter(attn_part.astype(jnp.bfloat16), 'tp', scatter_dimension=...  19.6 us
    all_gather x1, blocking collectives, local(): lax.all_gather(mixed, 'kv', axis=0, tiled=True)  13.1 us
    psum x1, blocking collectives, local(): total_squares = lax.psum(local_squares, 'kv')  12.4 us
    psum x1, blocking collectives, local(): mlp_total_squares = lax.psum(mlp_local_squares, 'kv')  11.7 us
    all_gather x1, blocking collectives, local(): lax.all_gather(stream, 'tp', axis=1, tiled=True).astype(jnp.float32)  6.6 us
  transfers between devices with their start and end apart: 4, of which 4 were waited for; matrix products, arithmetic and copies ran while one was open for 0% of the time, Pallas kernels for 0%

commit v1 on v0

--- a/solution.py
+++ b/solution.py
@@ -1,6 +1,11 @@
+import functools
+import math
+
 import jax
 import jax.numpy as jnp
 from jax import lax
+from jax.experimental import pallas as pl
+from jax.experimental.pallas import tpu as pltpu
 from jax.sharding import PartitionSpec as P
 
 D = 4096
@@ -122,9 +127,460 @@
     return (next_stream, new_state)
 
 
+LANES = 128
+VMEM_BYTES = 67043328
+MESH = pl.DeviceIdType.MESH
+
+
+def send_slots(count, axis, me, source, slots, send_sem, recv_sem):
+    copies = []
+    for step in range(1, count):
+        peer = lax.rem(me + step, count)
+        copy = pltpu.make_async_remote_copy(
+            src_ref=source(peer),
+            dst_ref=slots.at[me],
+            send_sem=send_sem.at[step],
+            recv_sem=recv_sem.at[step],
+            device_id={axis: peer},
+            device_id_type=MESH,
+        )
+        copy.start()
+        copies.append(copy)
+    return copies
+
+
+def wait_slot(count, axis, me, step, slots, send_sem, recv_sem):
+    origin = lax.rem(me + count - step, count)
+    pltpu.make_async_remote_copy(
+        src_ref=slots.at[origin],
+        dst_ref=slots.at[origin],
+        send_sem=send_sem.at[step],
+        recv_sem=recv_sem.at[step],
+        device_id={axis: origin},
+        device_id_type=MESH,
+    ).wait_recv()
+    return origin
+
+
+def layer_kernel(
+    kv_count,
+    tp_count,
+    stream,
+    attn_gain,
+    mlp_gain,
+    w_query,
+    w_key,
+    w_value,
+    w_zgate,
+    w_decay,
+    w_beta,
+    decay_rate,
+    head_gain,
+    w_attn_out,
+    w_gate,
+    w_up,
+    w_down,
+    state,
+    out_stream,
+    out_state,
+    v_query,
+    v_key,
+    v_value,
+    v_zgate,
+    v_decay,
+    v_beta,
+    v_attn_out,
+    v_gate,
+    v_up,
+    v_down,
+    v_state,
+    x_all,
+    normed,
+    proj_f,
+    proj_b,
+    proj_r,
+    proj_t,
+    rows,
+    mix_all,
+    mixed_f,
+    part_f,
+    part_b,
+    part_r,
+    res_all,
+    gu_f,
+    gu_b,
+    gu_r,
+    gu_t,
+    hid_all,
+    hidden_f,
+    down_f,
+    down_b,
+    down_r,
+    load_sem,
+    send_sem,
+    recv_sem,
+):
+    f32, bf16 = jnp.float32, jnp.bfloat16
+    kv, tp = lax.axis_index("kv"), lax.axis_index("tp")
+    batch, width = stream.shape
+    depth, cols = w_query.shape
+    seqs, heads = state.shape[0], state.shape[1]
+    heads_total = w_decay.shape[1]
+    half = w_gate.shape[1] // 2
+    features = kv_count * depth
+
+    def load(index, source, target):
+        copy = pltpu.make_async_copy(source, target, load_sem.at[index])
+        copy.start()
+        return copy
+
+    load_x = load(0, stream, x_all.at[tp])
+    loads = [
+        load(index + 1, source, target)
+        for index, (source, target) in enumerate(
+            (
+                (w_decay, v_decay),
+                (w_beta, v_beta),
+                (w_query, v_query),
+                (w_key, v_key),
+                (w_value, v_value),
+                (w_zgate, v_zgate),
+                (state, v_state),
+                (w_attn_out, v_attn_out),
+                (w_gate, v_gate),
+                (w_up, v_up),
+                (w_down, v_down),
+            )
+        )
+    ]
+    (l_decay, l_beta, l_query, l_key, l_value, l_zgate) = loads[:6]
+    (l_state, l_attn_out, l_gate, l_up, l_down) = loads[6:]
+
+    barrier = pltpu.get_barrier_semaphore()
+    for step in range(1, tp_count):
+        pl.semaphore_signal(
+            barrier, inc=1, device_id={"tp": lax.rem(tp + step, tp_count)}, device_id_type=MESH
+        )
+    for step in range(1, kv_count):
+        pl.semaphore_signal(
+            barrier, inc=1, device_id={"kv": lax.rem(kv + step, kv_count)}, device_id_type=MESH
+        )
+    load_x.wait()
+    pl.semaphore_wait(barrier, tp_count - 1 + kv_count - 1)
+
+    def tp_exchange(index, source, slots):
+        sends = send_slots(
+            tp_count, "tp", tp, source, slots, send_sem.at[index], recv_sem.at[index]
+        )
+
+        def arrived(step):
+            return wait_slot(
+                tp_count, "tp", tp, step, slots, send_sem.at[index], recv_sem.at[index]
+            )
+
+        return sends, arrived
+
+    def kv_exchange(index, source, slots):
+        sends = send_slots(
+            kv_count, "kv", kv, source, slots, send_sem.at[index], recv_sem.at[index]
+        )
+
+        def arrived(step):
+            return wait_slot(
+                kv_count, "kv", kv, step, slots, send_sem.at[index], recv_sem.at[index]
+            )
+
+        return sends, arrived
+
+    pending = []
+
+    def norm_inputs(blocks, gain):
+        squares = jnp.zeros((batch, 1), f32)
+        for t in range(tp_count):
+            block = blocks[t].astype(f32)
+            squares = squares + jnp.sum(block * block, axis=1, keepdims=True)
+            normed[:, t * width : (t + 1) * width] = (
+                block * gain[:, t * width : (t + 1) * width].astype(f32)
+            ).astype(bf16)
+        squares = jnp.broadcast_to(squares, (batch, LANES))
+        high = squares.astype(bf16).astype(f32)
+        return high, squares - high
+
+    sends, arrived = tp_exchange(0, lambda peer: x_all.at[tp], x_all)
+    pending += sends
+    for step in range(1, tp_count):
+        arrived(step)
+    high, low = norm_inputs(x_all, attn_gain)
+
+    inputs = normed[...]
+    l_decay.wait()
+    l_beta.wait()
+    decay_part = jnp.dot(inputs, v_decay[...], preferred_element_type=f32)
+    beta_part = jnp.dot(inputs, v_beta[...], preferred_element_type=f32)
+    for j in range(kv_count):
+        own = slice(j * seqs, (j + 1) * seqs)
+        proj_f[j, :, cols:] = jnp.zeros((4 * seqs, LANES), f32)
+        proj_f[j, 0:seqs, cols : cols + heads_total] = decay_part[own]
+        proj_f[j, seqs : 2 * seqs, cols : cols + heads_total] = beta_part[own]
+        proj_f[j, 2 * seqs : 3 * seqs, cols:] = high[own]
+        proj_f[j, 3 * seqs : 4 * seqs, cols:] = low[own]
+    for kind, (wait, weight) in enumerate(
+        ((l_query, v_query), (l_key, v_key), (l_value, v_value), (l_zgate, v_zgate))
+    ):
+        wait.wait()
+        part = jnp.dot(inputs, weight[...], preferred_element_type=f32)
+        for j in range(kv_count):
+            proj_f[j, kind * seqs : (kind + 1) * seqs, 0:cols] = part[j * seqs : (j + 1) * seqs]
+    for j in range(kv_count):
+        proj_b[j] = proj_f[j].astype(bf16)
+    sends, arrived = kv_exchange(1, lambda peer: proj_b.at[peer], proj_r)
+    pending += sends
+    total = proj_f[kv]
+    for step in range(1, kv_count):
+        total = total + proj_r[arrived(step)].astype(f32)
+    proj_t[...] = total
+
+    squares = proj_t[2 * seqs : 3 * seqs, cols:] + proj_t[3 * seqs : 4 * seqs, cols:]
+    row_scale = lax.rsqrt(squares / features + EPSILON)
+    decay_rows = proj_t[0:seqs, cols:] * row_scale
+    beta_rows = proj_t[seqs : 2 * seqs, cols:] * row_scale
+    for h in range(heads):
+        at = slice(h * seqs, (h + 1) * seqs)
+        for kind in range(4):
+            rows[kind, at, :] = (
+                proj_t[kind * seqs : (kind + 1) * seqs, h * LANES : (h + 1) * LANES] * row_scale
+            )
+        rows[4, at, :] = decay_rows
+        rows[5, at, :] = beta_rows
+    count = heads * seqs
+    row = lax.broadcasted_iota(jnp.int32, (count, LANES), 0)
+    lane = lax.broadcasted_iota(jnp.int32, (count, LANES), 1) - tp * heads
+    own_lane = (row >= lane * seqs) & (row < (lane + 1) * seqs)
+    decay_pre = jnp.sum(jnp.where(own_lane, rows[4], 0.0), axis=1, keepdims=True)
+    beta_pre = jnp.sum(jnp.where(own_lane, rows[5], 0.0), axis=1, keepdims=True)
+    row = lax.broadcasted_iota(jnp.int32, (count, heads), 0)
+    lane = lax.broadcasted_iota(jnp.int32, (count, heads), 1)
+    own_lane = (row >= lane * seqs) & (row < (lane + 1) * seqs)
+    rate = jnp.sum(
+        jnp.where(own_lane, jnp.broadcast_to(decay_rate[...], (count, heads)), 0.0),
+        axis=1,
+        keepdims=True,
+    )
+    softplus = jnp.maximum(decay_pre, 0.0) + jnp.log1p(jnp.exp(-jnp.abs(decay_pre)))
+    rows[4] = jnp.broadcast_to(jnp.exp(-rate * softplus), (count, LANES))
+    rows[5] = jnp.broadcast_to(jax.nn.sigmoid(beta_pre), (count, LANES))
+    query_t = jnp.transpose(l2_unit(rows[0]) * HEAD_DIM ** (-0.5))
+    key_t = jnp.transpose(l2_unit(rows[1]))
+
+    l_state.wait()
+    for h in range(heads):
+        for s in range(seqs):
+            i = h * seqs + s
+            key_col = key_t[:, i : i + 1]
+            decayed = v_state[s, h] * rows[4, i : i + 1, :]
+            recalled = jnp.sum(decayed * key_col, axis=0, keepdims=True)
+            update = rows[5, i : i + 1, :] * (rows[2, i : i + 1, :] - recalled)
+            updated = decayed + key_col * update
+            v_state[s, h] = updated
+            rows[0, i : i + 1, :] = jnp.sum(
+                updated * query_t[:, i : i + 1], axis=0, keepdims=True
+            )
+    head_out = rows[0]
+    scaled = head_out * lax.rsqrt(
+        jnp.mean(head_out * head_out, axis=-1, keepdims=True) + EPSILON
+    )
+    mix_all[kv] = (scaled * head_gain[...] * jax.nn.silu(rows[3])).astype(bf16)
+    sends, arrived = kv_exchange(2, lambda peer: mix_all.at[kv], mix_all)
+    pending += sends
+    store_state = pltpu.make_async_copy(v_state, out_state, load_sem.at[len(loads) + 1])
+    store_state.start()
+    for step in range(1, kv_count):
+        arrived(step)
+    for j in range(kv_count):
+        mixed = mix_all[j].astype(f32)
+        for h in range(heads):
+            mixed_f[j * seqs : (j + 1) * seqs, h * LANES : (h + 1) * LANES] = mixed[
+                h * seqs : (h + 1) * seqs
+            ]
+
+    def sum_over_tp(index, part, held, sent, slots):
+        for t in range(tp_count):
+            block = part[:, t * width : (t + 1) * width]
+            held[t] = block
+            sent[t] = block.astype(bf16)
+        sends, arrived = tp_exchange(index, lambda peer: sent.at[peer], slots)
+        total = held[tp]
+        for step in range(1, tp_count):
+            total = total + slots[arrived(step)].astype(f32)
+        return sends, total
+
+    l_attn_out.wait()
+    part = jnp.dot(mixed_f[...].astype(bf16), v_attn_out[...], preferred_element_type=f32)
+    sends, attn_sum = sum_over_tp(3, part, part_f, part_b, part_r)
+    pending += sends
+    res_all[tp] = (x_all[tp].astype(f32) + attn_sum).astype(bf16)
+    sends, arrived = tp_exchange(4, lambda peer: res_all.at[tp], res_all)
+    pending += sends
+    for step in range(1, tp_count):
+        arrived(step)
+    high, low = norm_inputs(res_all, mlp_gain)
+
+    inputs = normed[...]
+    for j in range(kv_count):
+        own = slice(j * seqs, (j + 1) * seqs)
+        gu_f[j, :, half:] = jnp.zeros((4 * seqs, LANES), f32)
+        gu_f[j, 0:seqs, half:] = high[own]
+        gu_f[j, seqs : 2 * seqs, half:] = low[own]
+    for kind, (wait, weight) in enumerate(((l_gate, v_gate), (l_up, v_up))):
+        wait.wait()
+        for side in range(2):
+            part = jnp.dot(
+                inputs,
+                weight[:, side * half : (side + 1) * half],
+                preferred_element_type=f32,
+            )
+            at = (2 * kind + side) * seqs
+            for j in range(kv_count):
+                gu_f[j, at : at + seqs, 0:half] = part[j * seqs : (j + 1) * seqs]
+    for j in range(kv_count):
+        gu_b[j] = gu_f[j].astype(bf16)
+    sends, arrived = kv_exchange(5, lambda peer: gu_b.at[peer], gu_r)
+    pending += sends
+    total = gu_f[kv]
+    for step in range(1, kv_count):
+        total = total + gu_r[arrived(step)].astype(f32)
+    gu_t[...] = total
+    squares = gu_t[0:seqs, half:] + gu_t[seqs : 2 * seqs, half:]
+    mlp_scale = lax.rsqrt(squares / features + EPSILON)[:, 0:1]
+    mlp_scale = jnp.concatenate([mlp_scale, mlp_scale], axis=0)
+    gate = gu_t[0 : 2 * seqs, 0:half] * mlp_scale
+    up = gu_t[2 * seqs : 4 * seqs, 0:half] * mlp_scale
+    hid_all[kv] = (jax.nn.silu(gate) * up).astype(bf16)
+    sends, arrived = kv_exchange(6, lambda peer: hid_all.at[kv], hid_all)
+    pending += sends
+    for step in range(1, kv_count):
+        arrived(step)
+    for j in range(kv_count):
+        hidden = hid_all[j].astype(f32)
+        for side in range(2):
+            hidden_f[j * seqs : (j + 1) * seqs, side * half : (side + 1) * half] = hidden[
+                side * seqs : (side + 1) * seqs
+            ]
+    l_down.wait()
+    part = jnp.dot(hidden_f[...].astype(bf16), v_down[...], preferred_element_type=f32)
+    sends, mlp_sum = sum_over_tp(7, part, down_f, down_b, down_r)
+    pending += sends
+    out_stream[...] = (res_all[tp].astype(f32) + mlp_sum).astype(bf16)
+    for copy in pending:
+        copy.wait_send()
+    store_state.wait()
+
+
+def fused(kv_count, tp_count, *args):
+    f32, bf16 = jnp.float32, jnp.bfloat16
+    (stream, attn_gain, mlp_gain, w_query, w_key, w_value, w_zgate, w_decay, w_beta) = args[:9]
+    (decay_rate, head_gain, w_attn_out, w_gate, w_up, w_down, state) = args[9:]
+    batch, width = stream.shape
+    depth, cols = w_query.shape
+    seqs, heads = state.shape[0], state.shape[1]
+    half = w_gate.shape[1] // 2
+    count = seqs * heads
+    steps = max(kv_count, tp_count)
+    any_spec = pl.BlockSpec(memory_space=pl.ANY)
+    vmem_spec = pl.BlockSpec(memory_space=pltpu.VMEM)
+    weights = (w_query, w_key, w_value, w_zgate, w_decay, w_beta, w_attn_out, w_gate, w_up, w_down)
+    scratch = [pltpu.VMEM(weight.shape, weight.dtype) for weight in weights + (state,)]
+    scratch += [
+        pltpu.VMEM((tp_count, batch, width), bf16),
+        pltpu.VMEM((batch, depth), bf16),
+        pltpu.VMEM((kv_count, 4 * seqs, cols + LANES), f32),
+        pltpu.VMEM((kv_count, 4 * seqs, cols + LANES), bf16),
+        pltpu.VMEM((kv_count, 4 * seqs, cols + LANES), bf16),
+        pltpu.VMEM((4 * seqs, cols + LANES), f32),
+        pltpu.VMEM((6, count, LANES), f32),
+        pltpu.VMEM((kv_count, count, LANES), bf16),
+        pltpu.VMEM((batch, cols), f32),
+        pltpu.VMEM((tp_count, batch, width), f32),
+        pltpu.VMEM((tp_count, batch, width), bf16),
+        pltpu.VMEM((tp_count, batch, width), bf16),
+        pltpu.VMEM((tp_count, batch, width), bf16),
+        pltpu.VMEM((kv_count, 4 * seqs, half + LANES), f32),
+        pltpu.VMEM((kv_count, 4 * seqs, half + LANES), bf16),
+        pltpu.VMEM((kv_count, 4 * seqs, half + LANES), bf16),
+        pltpu.VMEM((4 * seqs, half + LANES), f32),
+        pltpu.VMEM((kv_count, 2 * seqs, half), bf16),
+        pltpu.VMEM((batch, 2 * half), f32),
+        pltpu.VMEM((tp_count, batch, width), f32),
+        pltpu.VMEM((tp_count, batch, width), bf16),
+        pltpu.VMEM((tp_count, batch, width), bf16),
+        pltpu.SemaphoreType.DMA((13,)),
+        pltpu.SemaphoreType.DMA((8, steps)),
+        pltpu.SemaphoreType.DMA((8, steps)),
+    ]
+    return pl.pallas_call(
+        functools.partial(layer_kernel, kv_count, tp_count),
+        out_shape=(
+            jax.ShapeDtypeStruct(stream.shape, bf16),
+            jax.ShapeDtypeStruct(state.shape, f32),
+        ),
+        in_specs=[any_spec]
+        + [vmem_spec] * 2
+        + [any_spec] * 6
+        + [vmem_spec] * 2
+        + [any_spec] * 5,
+        out_specs=(vmem_spec, any_spec),
+        scratch_shapes=scratch,
+        compiler_params=pltpu.CompilerParams(
+            collective_id=0, has_side_effects=True, vmem_limit_bytes=VMEM_BYTES
+        ),
+    )(
+        stream,
+        attn_gain.reshape(1, -1),
+        mlp_gain.reshape(1, -1),
+        w_query,
+        w_key,
+        w_value,
+        w_zgate,
+        w_decay,
+        w_beta,
+        decay_rate.reshape(1, -1),
+        head_gain.reshape(1, -1),
+        w_attn_out,
+        w_gate,
+        w_up,
+        w_down,
+        state,
+    )
+
+
+def layer(mesh, *args):
+    kv_count, tp_count = mesh.shape["kv"], mesh.shape["tp"]
+    stream, w_query, w_gate, state = args[0], args[3], args[12], args[15]
+    seqs, heads = state.shape[0], state.shape[1]
+    held = sum(math.prod(a.shape) * a.dtype.itemsize for a in args)
+    tiled = (
+        stream.shape[1] % LANES == 0
+        and w_query.shape[0] == tp_count * stream.shape[1]
+        and stream.shape[0] == kv_count * seqs
+        and stream.shape[0] % 16 == 0
+        and (2 * seqs) % 8 == 0
+        and (seqs * heads) % 16 == 0
+        and w_gate.shape[1] % (2 * LANES) == 0
+        and args[7].shape[1] <= LANES
+        and state.shape[2] == LANES
+        and state.shape[3] == LANES
+        and kv_count > 1
+        and tp_count > 1
+        and held < VMEM_BYTES * 3 // 4
+    )
+    if tiled:
+        return fused(kv_count, tp_count, *args)
+    return local(*args)
+
+
 def solution(mesh):
     return jax.shard_map(
-        local,
+        functools.partial(layer, mesh),
         mesh=mesh,
         in_specs=(
             P("grp", ("kv", "tp")),

time: 190 us -> 54.5 us (0.29)
  waiting for transfers between devices: 94 us -> 0 us
  blocking collectives: 49 us -> 0 us
  Pallas kernels: 0 us -> 43.2 us
  matrix products: 22.3 us -> 0 us
  between operations: 14.6 us -> 0.64 us
  local copies, waits for them, and re-layouts: 4.03 us -> 10.4 us
  other arithmetic: 5.53 us -> 0 us
    pallas_call x0 -> x1, Pallas kernels: none -> 43.2 us  [fused(): pl.pallas_call(functools.partial(layer_kernel, kv_count, tp_count), out_s...]
    reduce_scatter x2 -> x0, waiting for transfers between devices: 39.4 us -> none  [the longest x1 19.8 us: local(): lax.psum_scatter(down_part.astype(jnp.bfloat16), 'tp', scatter_dimension=...]
    psum x1 -> x0, waiting for transfers between devices: 32.1 us -> none  [local(): lax.psum(operands[1].astype(jnp.bfloat16), 'kv').astype(jnp.float32)]
    all_gather x3 -> x0, blocking collectives: 24.9 us -> none  [the longest x1 13.1 us: local(): lax.all_gather(mixed, 'kv', axis=0, tiled=True)]
    psum x2 -> x0, blocking collectives: 24.1 us -> none  [the longest x1 12.4 us: local(): total_squares = lax.psum(local_squares, 'kv')]
    unnamed x5 -> x0, waiting for transfers between devices: 22.5 us -> none
    dot_general x11 -> x0, matrix products: 22.3 us -> none  [the longest x1 4.26 us: local(): down_part = jnp.dot(hidden, w_down, preferred_element_type=jnp.float32)]
    unnamed x30 -> x4, local copies, waits for them, and re-layouts: 3.11 us -> 7.83 us
  transfers between devices with their start and end apart: 4 -> 0, of which waited for: 4 -> 0; matrix products, arithmetic and copies ran while one was open for 0% -> 0% of each run, Pallas kernels for 0% -> 0%
where the time goes in v1:
time: 54.5 us; the launch traced here: 54.2 us
  Pallas kernels  43.2 us (79%)
  local copies, waits for them, and re-layouts  10.4 us (19%)
  between operations  0.64 us (1%)
    pallas_call x1, Pallas kernels, fused(): pl.pallas_call(functools.partial(layer_kernel, kv_count, tp_count), out_s...  43.2 us
    unnamed x4, local copies, waits for them, and re-layouts  7.83 us
    reshape x1, local copies, waits for them, and re-layouts, fused(): attn_gain.reshape(1, -1)  1.28 us
    reshape x1, local copies, waits for them, and re-layouts, fused(): mlp_gain.reshape(1, -1)  1.28 us

profile of v1, /device:TPU:0, one launch (start us, length us, event | category | flops | bytes accessed | tf_op | source)
XLA Modules:
  0.0 54.2 jit_solution(8205591222369833184)
XLA Ops:
  0.6 1.3 %reshape.16.attn_gain = bf16[1,1024]{1,0:T(2,128)(2,1)} reshape(bf16[1024]{0:T(1024)(128)(2,1)} %param.17) | data formatting | bytes 4096 | tf_op jit(solution)/shard_map/reshape | solution.py:538
  1.9 1.3 %reshape.17.mlp_gain = bf16[1,1024]{1,0:T(2,128)(2,1)} reshape(bf16[1024]{0:T(1024)(128)(2,1)} %param.18) | data formatting | bytes 4096 | tf_op jit(solution)/shard_map/reshape | solution.py:539
  3.2 1.7 %copy.18.w_decay = bf16[1024,32]{1,0:T(8,128)(2,1)} copy(bf16[1024,32]{0,1:T(8,128)(2,1)} %param.23) | data formatting | bytes 131072 | tf_op args[7]
  4.9 1.7 %copy.19.w_beta = bf16[1024,32]{1,0:T(8,128)(2,1)} copy(bf16[1024,32]{0,1:T(8,128)(2,1)} %param.24) | data formatting | bytes 131072 | tf_op args[8]
  6.6 43.2 %shard_map.167 = (bf16[16,256]{1,0:T(8,128)(2,1)}, f32[4,8,128,128]{3,2,1,0:T(8,128)}) custom-call(bf16[16,256]{1,0:T(8,128)(2,1)} %stream.1, bf16[1,1024]{1,0:T(2,128)(2,1)} %reshape.16.attn_gain, bf16[1,1024]{1,0:T(2,128)(2,1)} %reshape.17.mlp_gain, bf16[1024,1024]{1,0:T(8,128)(2,1)} %w_query.1, bf16[1024,1024]{1,0:T(8,128)(2,1)} %w_key.1, ...), custom_call_target="tpu_custom_call" | custom-call | tf_op jit(solution)/shard_map/pallas_call | solution.py:520
  49.7 1.3 %copy.22 = bf16[16,256]{1,0:T(8,128)(2,1)} copy(bf16[16,256]{1,0:T(8,128)(2,1)} %get-tuple-element.4) | data formatting | bytes 16384
  51.0 3.1 %copy.23 = f32[4,8,128,128]{3,2,1,0:T(8,128)} copy(f32[4,8,128,128]{3,2,1,0:T(8,128)} %get-tuple-element.5) | data formatting | bytes 4194304

commit v2 on v1

--- a/solution.py
+++ b/solution.py
@@ -129,6 +129,7 @@
 
 LANES = 128
 VMEM_BYTES = 67043328
+LIMIT = 40 * 1024 * 1024
 MESH = pl.DeviceIdType.MESH
 
 
@@ -216,6 +217,7 @@
     down_f,
     down_b,
     down_r,
+    next_stream,
     load_sem,
     send_sem,
     recv_sem,
@@ -225,7 +227,7 @@
     batch, width = stream.shape
     depth, cols = w_query.shape
     seqs, heads = state.shape[0], state.shape[1]
-    heads_total = w_decay.shape[1]
+    heads_total = w_decay.shape[0]
     half = w_gate.shape[1] // 2
     features = kv_count * depth
 
@@ -299,9 +301,10 @@
         for t in range(tp_count):
             block = blocks[t].astype(f32)
             squares = squares + jnp.sum(block * block, axis=1, keepdims=True)
-            normed[:, t * width : (t + 1) * width] = (
-                block * gain[:, t * width : (t + 1) * width].astype(f32)
-            ).astype(bf16)
+            for c in range(0, width, LANES):
+                at = t * width + c
+                scale = gain[...].astype(f32)[at // LANES : at // LANES + 1]
+                normed[:, at : at + LANES] = (block[:, c : c + LANES] * scale).astype(bf16)
         squares = jnp.broadcast_to(squares, (batch, LANES))
         high = squares.astype(bf16).astype(f32)
         return high, squares - high
@@ -315,8 +318,9 @@
     inputs = normed[...]
     l_decay.wait()
     l_beta.wait()
-    decay_part = jnp.dot(inputs, v_decay[...], preferred_element_type=f32)
-    beta_part = jnp.dot(inputs, v_beta[...], preferred_element_type=f32)
+    by_rows = (((1,), (1,)), ((), ()))
+    decay_part = lax.dot_general(inputs, v_decay[...], by_rows, preferred_element_type=f32)
+    beta_part = lax.dot_general(inputs, v_beta[...], by_rows, preferred_element_type=f32)
     for j in range(kv_count):
         own = slice(j * seqs, (j + 1) * seqs)
         proj_f[j, :, cols:] = jnp.zeros((4 * seqs, LANES), f32)
@@ -470,7 +474,10 @@
     part = jnp.dot(hidden_f[...].astype(bf16), v_down[...], preferred_element_type=f32)
     sends, mlp_sum = sum_over_tp(7, part, down_f, down_b, down_r)
     pending += sends
-    out_stream[...] = (res_all[tp].astype(f32) + mlp_sum).astype(bf16)
+    next_stream[...] = (res_all[tp].astype(f32) + mlp_sum).astype(bf16)
+    store_stream = pltpu.make_async_copy(next_stream, out_stream, load_sem.at[0])
+    store_stream.start()
+    store_stream.wait()
     for copy in pending:
         copy.wait_send()
     store_state.wait()
@@ -486,9 +493,10 @@
     half = w_gate.shape[1] // 2
     count = seqs * heads
     steps = max(kv_count, tp_count)
-    any_spec = pl.BlockSpec(memory_space=pl.ANY)
+    any_spec = pl.BlockSpec(memory_space=pltpu.HBM)
     vmem_spec = pl.BlockSpec(memory_space=pltpu.VMEM)
-    weights = (w_query, w_key, w_value, w_zgate, w_decay, w_beta, w_attn_out, w_gate, w_up, w_down)
+    small = jax.ShapeDtypeStruct(w_decay.shape[::-1], w_decay.dtype)
+    weights = (w_query, w_key, w_value, w_zgate, small, small, w_attn_out, w_gate, w_up, w_down)
     scratch = [pltpu.VMEM(weight.shape, weight.dtype) for weight in weights + (state,)]
     scratch += [
         pltpu.VMEM((tp_count, batch, width), bf16),
@@ -513,36 +521,35 @@
         pltpu.VMEM((tp_count, batch, width), f32),
         pltpu.VMEM((tp_count, batch, width), bf16),
         pltpu.VMEM((tp_count, batch, width), bf16),
+        pltpu.VMEM((batch, width), bf16),
         pltpu.SemaphoreType.DMA((13,)),
         pltpu.SemaphoreType.DMA((8, steps)),
         pltpu.SemaphoreType.DMA((8, steps)),
     ]
-    return pl.pallas_call(
+    outs = pl.pallas_call(
         functools.partial(layer_kernel, kv_count, tp_count),
-        out_shape=(
-            jax.ShapeDtypeStruct(stream.shape, bf16),
-            jax.ShapeDtypeStruct(state.shape, f32),
-        ),
+        out_shape=(pltpu.VMEM(stream.shape, bf16), pltpu.VMEM(state.shape, f32)),
         in_specs=[any_spec]
         + [vmem_spec] * 2
         + [any_spec] * 6
         + [vmem_spec] * 2
         + [any_spec] * 5,
-        out_specs=(vmem_spec, any_spec),
+        out_specs=(pl.BlockSpec(memory_space=pl.ANY),) * 2,
         scratch_shapes=scratch,
         compiler_params=pltpu.CompilerParams(
-            collective_id=0, has_side_effects=True, vmem_limit_bytes=VMEM_BYTES
+            collective_id=0, has_side_effects=True, vmem_limit_bytes=LIMIT
         ),
     )(
+        *map(in_hbm, (
         stream,
-        attn_gain.reshape(1, -1),
-        mlp_gain.reshape(1, -1),
+        attn_gain.reshape(-1, LANES),
+        mlp_gain.reshape(-1, LANES),
         w_query,
         w_key,
         w_value,
         w_zgate,
-        w_decay,
-        w_beta,
+        w_decay.T,
+        w_beta.T,
         decay_rate.reshape(1, -1),
         head_gain.reshape(1, -1),
         w_attn_out,
@@ -550,7 +557,31 @@
         w_up,
         w_down,
         state,
-    )
+        ))
+    )
+    return pl.pallas_call(
+        finish_kernel,
+        out_shape=tuple(jax.ShapeDtypeStruct(out.shape, out.dtype) for out in outs),
+        in_specs=[pl.BlockSpec(memory_space=pl.ANY)] * 2,
+        out_specs=(any_spec,) * 2,
+        scratch_shapes=[pltpu.SemaphoreType.DMA((2,))],
+        compiler_params=pltpu.CompilerParams(vmem_limit_bytes=1024 * 1024),
+    )(*outs)
+
+
+def in_hbm(array):
+    return pltpu.with_memory_space_constraint(array, pltpu.HBM)
+
+
+def finish_kernel(stream, state, out_stream, out_state, sem):
+    copies = [
+        pltpu.make_async_copy(state, out_state, sem.at[0]),
+        pltpu.make_async_copy(stream, out_stream, sem.at[1]),
+    ]
+    for copy in copies:
+        copy.start()
+    for copy in copies:
+        copy.wait()
 
 
 def layer(mesh, *args):

time: 54.5 us -> 44.8 us (0.82)
  local copies, waits for them, and re-layouts: 10.4 us -> 0 us
  Pallas kernels: 43.2 us -> 43.9 us
    unnamed x4 -> x0, local copies, waits for them, and re-layouts: 7.83 us -> none
    reshape x2 -> x0, local copies, waits for them, and re-layouts: 2.55 us -> none  [the longest x1 1.28 us: fused(): attn_gain.reshape(1, -1)]
    pallas_call x0 -> x1, Pallas kernels: none -> 1.34 us  [fused(): pl.pallas_call(finish_kernel, out_shape=tuple((jax.ShapeDtypeStruct(out.s...]
    pallas_call x1, Pallas kernels: 43.2 us -> 42.6 us  [fused(): pl.pallas_call(functools.partial(layer_kernel, kv_count, tp_count), out_s...]
where the time goes in v2:
time: 44.8 us; the launch traced here: 44.6 us
  Pallas kernels  43.9 us (98%)
  between operations  0.64 us (1%)
    pallas_call x1, Pallas kernels, fused(): pl.pallas_call(functools.partial(layer_kernel, kv_count, tp_count), out_s...  42.6 us
    pallas_call x1, Pallas kernels, fused(): pl.pallas_call(finish_kernel, out_shape=tuple((jax.ShapeDtypeStruct(out.s...  1.34 us

profile of v2, /device:TPU:0, one launch (start us, length us, event | category | flops | bytes accessed | tf_op | source)
XLA Modules:
  0.0 44.6 jit_solution(15738222283670269938)
XLA Ops:
  0.6 42.6 %shard_map.167 = (bf16[16,256]{1,0:T(8,128)(2,1)S(1)}, f32[4,8,128,128]{3,2,1,0:T(8,128)S(1)}) custom-call(bf16[16,256]{1,0:T(8,128)(2,1)} %stream.1, bf16[8,128]{1,0:T(8,128)(2,1)} %bitcast.8, bf16[8,128]{1,0:T(8,128)(2,1)} %bitcast.9, bf16[1024,1024]{1,0:T(8,128)(2,1)} %w_query.1, bf16[1024,1024]{1,0:T(8,128)(2,1)} %w_key.1, bf16[1024,1024]{1,0:T(8,128)(2,1)} %w_value.1, ...), custom_call_target="tpu_custom_call" | custom-call | tf_op jit(solution)/shard_map/pallas_call | solution.py:529
  43.2 1.3 %shard_map.168 = (bf16[16,256]{1,0:T(8,128)(2,1)}, f32[4,8,128,128]{3,2,1,0:T(8,128)}) custom-call(bf16[16,256]{1,0:T(8,128)(2,1)S(1)} %get-tuple-element.4.stream, f32[4,8,128,128]{3,2,1,0:T(8,128)S(1)} %get-tuple-element.5.state), custom_call_target="tpu_custom_call" | custom-call | tf_op jit(solution)/shard_map/pallas_call | solution.py:562

commit v3 on v2

--- a/solution.py
+++ b/solution.py
@@ -133,15 +133,22 @@
 MESH = pl.DeviceIdType.MESH
 
 
-def send_slots(count, axis, me, source, slots, send_sem, recv_sem):
+def partner(count, me, step):
+    upper = lax.div(2 * me, count)
+    falling = count - 1 - step - lax.div(me + step + 1, count)
+    rising = step + lax.div(step + count - me, count)
+    return upper * rising + (1 - upper) * falling
+
+
+def send_slots(count, axis, me, source, target, send_sem, recv_sem):
     copies = []
-    for step in range(1, count):
-        peer = lax.rem(me + step, count)
+    for step in range(count - 1):
+        peer = partner(count, me, step)
         copy = pltpu.make_async_remote_copy(
             src_ref=source(peer),
-            dst_ref=slots.at[me],
+            dst_ref=target(me),
             send_sem=send_sem.at[step],
-            recv_sem=recv_sem.at[step],
+            recv_sem=recv_sem.at[me],
             device_id={axis: peer},
             device_id_type=MESH,
         )
@@ -150,13 +157,13 @@
     return copies
 
 
-def wait_slot(count, axis, me, step, slots, send_sem, recv_sem):
-    origin = lax.rem(me + count - step, count)
+def wait_slot(count, axis, me, step, target, send_sem, recv_sem):
+    origin = partner(count, me, count - 2 - step)
     pltpu.make_async_remote_copy(
-        src_ref=slots.at[origin],
-        dst_ref=slots.at[origin],
+        src_ref=target(origin),
+        dst_ref=target(origin),
         send_sem=send_sem.at[step],
-        recv_sem=recv_sem.at[step],
+        recv_sem=recv_sem.at[origin],
         device_id={axis: origin},
         device_id_type=MESH,
     ).wait_recv()
@@ -204,9 +211,7 @@
     rows,
     mix_all,
     mixed_f,
-    part_f,
     part_b,
-    part_r,
     res_all,
     gu_f,
     gu_b,
@@ -218,6 +223,10 @@
     down_b,
     down_r,
     next_stream,
+    g_attn,
+    g_mlp,
+    v_rate,
+    g_head,
     load_sem,
     send_sem,
     recv_sem,
@@ -231,6 +240,16 @@
     half = w_gate.shape[1] // 2
     features = kv_count * depth
 
+    barrier = pltpu.get_barrier_semaphore()
+    for step in range(1, tp_count):
+        pl.semaphore_signal(
+            barrier, inc=1, device_id={"tp": lax.rem(tp + step, tp_count)}, device_id_type=MESH
+        )
+    for step in range(1, kv_count):
+        pl.semaphore_signal(
+            barrier, inc=1, device_id={"kv": lax.rem(kv + step, kv_count)}, device_id_type=MESH
+        )
+
     def load(index, source, target):
         copy = pltpu.make_async_copy(source, target, load_sem.at[index])
         copy.start()
@@ -241,6 +260,10 @@
         load(index + 1, source, target)
         for index, (source, target) in enumerate(
             (
+                (attn_gain, g_attn),
+                (mlp_gain, g_mlp),
+                (decay_rate, v_rate),
+                (head_gain, g_head),
                 (w_decay, v_decay),
                 (w_beta, v_beta),
                 (w_query, v_query),
@@ -255,46 +278,25 @@
             )
         )
     ]
-    (l_decay, l_beta, l_query, l_key, l_value, l_zgate) = loads[:6]
-    (l_state, l_attn_out, l_gate, l_up, l_down) = loads[6:]
-
-    barrier = pltpu.get_barrier_semaphore()
-    for step in range(1, tp_count):
-        pl.semaphore_signal(
-            barrier, inc=1, device_id={"tp": lax.rem(tp + step, tp_count)}, device_id_type=MESH
-        )
-    for step in range(1, kv_count):
-        pl.semaphore_signal(
-            barrier, inc=1, device_id={"kv": lax.rem(kv + step, kv_count)}, device_id_type=MESH
-        )
+    (l_decay, l_beta, l_query, l_key, l_value, l_zgate) = loads[4:10]
+    (l_state, l_attn_out, l_gate, l_up, l_down) = loads[10:]
+
     load_x.wait()
     pl.semaphore_wait(barrier, tp_count - 1 + kv_count - 1)
 
-    def tp_exchange(index, source, slots):
-        sends = send_slots(
-            tp_count, "tp", tp, source, slots, send_sem.at[index], recv_sem.at[index]
-        )
+    pending = []
+
+    def exchange(count, axis, me, index, source, target):
+        sems = send_sem.at[index], recv_sem.at[index]
+        pending.extend(send_slots(count, axis, me, source, target, *sems))
 
         def arrived(step):
-            return wait_slot(
-                tp_count, "tp", tp, step, slots, send_sem.at[index], recv_sem.at[index]
-            )
-
-        return sends, arrived
-
-    def kv_exchange(index, source, slots):
-        sends = send_slots(
-            kv_count, "kv", kv, source, slots, send_sem.at[index], recv_sem.at[index]
-        )
-
-        def arrived(step):
-            return wait_slot(
-                kv_count, "kv", kv, step, slots, send_sem.at[index], recv_sem.at[index]
-            )
-
-        return sends, arrived
-
-    pending = []
+            return wait_slot(count, axis, me, step, target, *sems)
+
+        return arrived
+
+    tp_exchange = functools.partial(exchange, tp_count, "tp", tp)
+    kv_exchange = functools.partial(exchange, kv_count, "kv", kv)
 
     def norm_inputs(blocks, gain):
         squares = jnp.zeros((batch, 1), f32)
@@ -309,11 +311,12 @@
         high = squares.astype(bf16).astype(f32)
         return high, squares - high
 
-    sends, arrived = tp_exchange(0, lambda peer: x_all.at[tp], x_all)
-    pending += sends
-    for step in range(1, tp_count):
+    arrived = tp_exchange(0, lambda peer: x_all.at[tp], lambda slot: x_all.at[slot])
+    for step in range(tp_count - 1):
         arrived(step)
-    high, low = norm_inputs(x_all, attn_gain)
+    for small in loads[:4]:
+        small.wait()
+    high, low = norm_inputs(x_all, g_attn)
 
     inputs = normed[...]
     l_decay.wait()
@@ -328,20 +331,32 @@
         proj_f[j, seqs : 2 * seqs, cols : cols + heads_total] = beta_part[own]
         proj_f[j, 2 * seqs : 3 * seqs, cols:] = high[own]
         proj_f[j, 3 * seqs : 4 * seqs, cols:] = low[own]
-    for kind, (wait, weight) in enumerate(
-        ((l_query, v_query), (l_key, v_key), (l_value, v_value), (l_zgate, v_zgate))
-    ):
-        wait.wait()
-        part = jnp.dot(inputs, weight[...], preferred_element_type=f32)
+    projections = ((l_query, v_query), (l_key, v_key), (l_value, v_value), (l_zgate, v_zgate))
+    arrivals = []
+    for side in range(2):
+        at = pl.ds(2 * side * seqs, 2 * seqs)
+        for kind in (2 * side, 2 * side + 1):
+            wait, weight = projections[kind]
+            wait.wait()
+            part = jnp.dot(inputs, weight[...], preferred_element_type=f32)
+            for j in range(kv_count):
+                proj_f[j, kind * seqs : (kind + 1) * seqs, 0:cols] = part[
+                    j * seqs : (j + 1) * seqs
+                ]
         for j in range(kv_count):
-            proj_f[j, kind * seqs : (kind + 1) * seqs, 0:cols] = part[j * seqs : (j + 1) * seqs]
-    for j in range(kv_count):
-        proj_b[j] = proj_f[j].astype(bf16)
-    sends, arrived = kv_exchange(1, lambda peer: proj_b.at[peer], proj_r)
-    pending += sends
+            proj_b[j, at] = proj_f[j, at].astype(bf16)
+        arrivals.append(
+            kv_exchange(
+                1 + side,
+                lambda peer, at=at: proj_b.at[peer, at],
+                lambda slot, at=at: proj_r.at[slot, at],
+            )
+        )
     total = proj_f[kv]
-    for step in range(1, kv_count):
-        total = total + proj_r[arrived(step)].astype(f32)
+    for step in range(kv_count - 1):
+        for arrived in arrivals:
+            origin = arrived(step)
+        total = total + proj_r[origin].astype(f32)
     proj_t[...] = total
 
     squares = proj_t[2 * seqs : 3 * seqs, cols:] + proj_t[3 * seqs : 4 * seqs, cols:]
@@ -366,7 +381,7 @@
     lane = lax.broadcasted_iota(jnp.int32, (count, heads), 1)
     own_lane = (row >= lane * seqs) & (row < (lane + 1) * seqs)
     rate = jnp.sum(
-        jnp.where(own_lane, jnp.broadcast_to(decay_rate[...], (count, heads)), 0.0),
+        jnp.where(own_lane, jnp.broadcast_to(v_rate[...], (count, heads)), 0.0),
         axis=1,
         keepdims=True,
     )
@@ -393,12 +408,11 @@
     scaled = head_out * lax.rsqrt(
         jnp.mean(head_out * head_out, axis=-1, keepdims=True) + EPSILON
     )
-    mix_all[kv] = (scaled * head_gain[...] * jax.nn.silu(rows[3])).astype(bf16)
-    sends, arrived = kv_exchange(2, lambda peer: mix_all.at[kv], mix_all)
-    pending += sends
+    mix_all[kv] = (scaled * g_head[...] * jax.nn.silu(rows[3])).astype(bf16)
+    arrived = kv_exchange(3, lambda peer: mix_all.at[kv], lambda slot: mix_all.at[slot])
     store_state = pltpu.make_async_copy(v_state, out_state, load_sem.at[len(loads) + 1])
     store_state.start()
-    for step in range(1, kv_count):
+    for step in range(kv_count - 1):
         arrived(step)
     for j in range(kv_count):
         mixed = mix_all[j].astype(f32)
@@ -407,27 +421,21 @@
                 h * seqs : (h + 1) * seqs
             ]
 
-    def sum_over_tp(index, part, held, sent, slots):
-        for t in range(tp_count):
-            block = part[:, t * width : (t + 1) * width]
-            held[t] = block
-            sent[t] = block.astype(bf16)
-        sends, arrived = tp_exchange(index, lambda peer: sent.at[peer], slots)
-        total = held[tp]
-        for step in range(1, tp_count):
-            total = total + slots[arrived(step)].astype(f32)
-        return sends, total
-
     l_attn_out.wait()
-    part = jnp.dot(mixed_f[...].astype(bf16), v_attn_out[...], preferred_element_type=f32)
-    sends, attn_sum = sum_over_tp(3, part, part_f, part_b, part_r)
-    pending += sends
-    res_all[tp] = (x_all[tp].astype(f32) + attn_sum).astype(bf16)
-    sends, arrived = tp_exchange(4, lambda peer: res_all.at[tp], res_all)
-    pending += sends
-    for step in range(1, tp_count):
+    part_b[tp] = jnp.dot(
+        mixed_f[...].astype(bf16), v_attn_out[...], preferred_element_type=f32
+    ).astype(bf16)
+    arrived = tp_exchange(4, lambda peer: part_b.at[tp], lambda slot: part_b.at[slot])
+    for step in range(tp_count - 1):
         arrived(step)
-    high, low = norm_inputs(res_all, mlp_gain)
+    total = part_b[0].astype(f32)
+    for t in range(1, tp_count):
+        total = total + part_b[t].astype(f32)
+    for t in range(tp_count):
+        res_all[t] = (
+            x_all[t].astype(f32) + total[:, t * width : (t + 1) * width]
+        ).astype(bf16)
+    high, low = norm_inputs(res_all, g_mlp)
 
     inputs = normed[...]
     for j in range(kv_count):
@@ -435,6 +443,7 @@
         gu_f[j, :, half:] = jnp.zeros((4 * seqs, LANES), f32)
         gu_f[j, 0:seqs, half:] = high[own]
         gu_f[j, seqs : 2 * seqs, half:] = low[own]
+    arrivals = []
     for kind, (wait, weight) in enumerate(((l_gate, v_gate), (l_up, v_up))):
         wait.wait()
         for side in range(2):
@@ -446,13 +455,21 @@
             at = (2 * kind + side) * seqs
             for j in range(kv_count):
                 gu_f[j, at : at + seqs, 0:half] = part[j * seqs : (j + 1) * seqs]
-    for j in range(kv_count):
-        gu_b[j] = gu_f[j].astype(bf16)
-    sends, arrived = kv_exchange(5, lambda peer: gu_b.at[peer], gu_r)
-    pending += sends
+        at = pl.ds(2 * kind * seqs, 2 * seqs)
+        for j in range(kv_count):
+            gu_b[j, at] = gu_f[j, at].astype(bf16)
+        arrivals.append(
+            kv_exchange(
+                5 + kind,
+                lambda peer, at=at: gu_b.at[peer, at],
+                lambda slot, at=at: gu_r.at[slot, at],
+            )
+        )
     total = gu_f[kv]
-    for step in range(1, kv_count):
-        total = total + gu_r[arrived(step)].astype(f32)
+    for step in range(kv_count - 1):
+        for arrived in arrivals:
+            origin = arrived(step)
+        total = total + gu_r[origin].astype(f32)
     gu_t[...] = total
     squares = gu_t[0:seqs, half:] + gu_t[seqs : 2 * seqs, half:]
     mlp_scale = lax.rsqrt(squares / features + EPSILON)[:, 0:1]
@@ -460,9 +477,8 @@
     gate = gu_t[0 : 2 * seqs, 0:half] * mlp_scale
     up = gu_t[2 * seqs : 4 * seqs, 0:half] * mlp_scale
     hid_all[kv] = (jax.nn.silu(gate) * up).astype(bf16)
-    sends, arrived = kv_exchange(6, lambda peer: hid_all.at[kv], hid_all)
-    pending += sends
-    for step in range(1, kv_count):
+    arrived = kv_exchange(7, lambda peer: hid_all.at[kv], lambda slot: hid_all.at[slot])
+    for step in range(kv_count - 1):
         arrived(step)
     for j in range(kv_count):
         hidden = hid_all[j].astype(f32)
@@ -472,8 +488,14 @@
             ]
     l_down.wait()
     part = jnp.dot(hidden_f[...].astype(bf16), v_down[...], preferred_element_type=f32)
-    sends, mlp_sum = sum_over_tp(7, part, down_f, down_b, down_r)
-    pending += sends
+    for t in range(tp_count):
+        block = part[:, t * width : (t + 1) * width]
+        down_f[t] = block
+        down_b[t] = block.astype(bf16)
+    arrived = tp_exchange(8, lambda peer: down_b.at[peer], lambda slot: down_r.at[slot])
+    mlp_sum = down_f[tp]
+    for step in range(tp_count - 1):
+        mlp_sum = mlp_sum + down_r[arrived(step)].astype(f32)
     next_stream[...] = (res_all[tp].astype(f32) + mlp_sum).astype(bf16)
     store_stream = pltpu.make_async_copy(next_stream, out_stream, load_sem.at[0])
     store_stream.start()
@@ -494,7 +516,6 @@
     count = seqs * heads
     steps = max(kv_count, tp_count)
     any_spec = pl.BlockSpec(memory_space=pltpu.HBM)
-    vmem_spec = pl.BlockSpec(memory_space=pltpu.VMEM)
     small = jax.ShapeDtypeStruct(w_decay.shape[::-1], w_decay.dtype)
     weights = (w_query, w_key, w_value, w_zgate, small, small, w_attn_out, w_gate, w_up, w_down)
     scratch = [pltpu.VMEM(weight.shape, weight.dtype) for weight in weights + (state,)]
@@ -508,9 +529,7 @@
         pltpu.VMEM((6, count, LANES), f32),
         pltpu.VMEM((kv_count, count, LANES), bf16),
         pltpu.VMEM((batch, cols), f32),
-        pltpu.VMEM((tp_count, batch, width), f32),
-        pltpu.VMEM((tp_count, batch, width), bf16),
-        pltpu.VMEM((tp_count, batch, width), bf16),
+        pltpu.VMEM((tp_count, batch, tp_count * width), bf16),
         pltpu.VMEM((tp_count, batch, width), bf16),
         pltpu.VMEM((kv_count, 4 * seqs, half + LANES), f32),
         pltpu.VMEM((kv_count, 4 * seqs, half + LANES), bf16),
@@ -522,18 +541,18 @@
         pltpu.VMEM((tp_count, batch, width), bf16),
         pltpu.VMEM((tp_count, batch, width), bf16),
         pltpu.VMEM((batch, width), bf16),
-        pltpu.SemaphoreType.DMA((13,)),
-        pltpu.SemaphoreType.DMA((8, steps)),
-        pltpu.SemaphoreType.DMA((8, steps)),
+        pltpu.VMEM((depth // LANES, LANES), bf16),
+        pltpu.VMEM((depth // LANES, LANES), bf16),
+        pltpu.VMEM((1, heads), f32),
+        pltpu.VMEM((1, LANES), f32),
+        pltpu.SemaphoreType.DMA((17,)),
+        pltpu.SemaphoreType.DMA((9, steps)),
+        pltpu.SemaphoreType.DMA((9, steps)),
     ]
     outs = pl.pallas_call(
         functools.partial(layer_kernel, kv_count, tp_count),
         out_shape=(pltpu.VMEM(stream.shape, bf16), pltpu.VMEM(state.shape, f32)),
-        in_specs=[any_spec]
-        + [vmem_spec] * 2
-        + [any_spec] * 6
-        + [vmem_spec] * 2
-        + [any_spec] * 5,
+        in_specs=[any_spec] * len(args),
         out_specs=(pl.BlockSpec(memory_space=pl.ANY),) * 2,
         scratch_shapes=scratch,
         compiler_params=pltpu.CompilerParams(
@@ -592,6 +611,7 @@
     tiled = (
         stream.shape[1] % LANES == 0
         and w_query.shape[0] == tp_count * stream.shape[1]
+        and args[11].shape[1] == tp_count * stream.shape[1]
         and stream.shape[0] == kv_count * seqs
         and stream.shape[0] % 16 == 0
         and (2 * seqs) % 8 == 0

time: 44.8 us -> 40.2 us (0.90)
  Pallas kernels: 43.9 us -> 39.4 us
    pallas_call x1, Pallas kernels: 42.6 us -> 38 us  [fused(): pl.pallas_call(functools.partial(layer_kernel, kv_count, tp_count), out_s...]
where the time goes in v3:
time: 40.2 us; the launch traced here: 40 us
  Pallas kernels  39.4 us (98%)
  between operations  0.64 us (2%)
    pallas_call x1, Pallas kernels, fused(): pl.pallas_call(functools.partial(layer_kernel, kv_count, tp_count), out_s...  38 us
    pallas_call x1, Pallas kernels, fused(): pl.pallas_call(finish_kernel, out_shape=tuple((jax.ShapeDtypeStruct(out.s...  1.34 us

profile of v3, /device:TPU:0, one launch (start us, length us, event | category | flops | bytes accessed | tf_op | source)
XLA Modules:
  0.0 40.0 jit_solution(11816656408228654542)
XLA Ops:
  0.6 38.0 %shard_map.167 = (bf16[16,256]{1,0:T(8,128)(2,1)S(1)}, f32[4,8,128,128]{3,2,1,0:T(8,128)S(1)}) custom-call(bf16[16,256]{1,0:T(8,128)(2,1)} %stream.1, bf16[8,128]{1,0:T(8,128)(2,1)} %bitcast.8, bf16[8,128]{1,0:T(8,128)(2,1)} %bitcast.9, bf16[1024,1024]{1,0:T(8,128)(2,1)} %w_query.1, bf16[1024,1024]{1,0:T(8,128)(2,1)} %w_key.1, bf16[1024,1024]{1,0:T(8,128)(2,1)} %w_value.1, ...), custom_call_target="tpu_custom_call" | custom-call | tf_op jit(solution)/shard_map/pallas_call | solution.py:552
  38.7 1.3 %shard_map.168 = (bf16[16,256]{1,0:T(8,128)(2,1)}, f32[4,8,128,128]{3,2,1,0:T(8,128)}) custom-call(bf16[16,256]{1,0:T(8,128)(2,1)S(1)} %get-tuple-element.4.stream, f32[4,8,128,128]{3,2,1,0:T(8,128)S(1)} %get-tuple-element.5.state), custom_call_target="tpu_custom_call" | custom-call | tf_op jit(solution)/shard_map/pallas_call | solution.py:581
